TPU v7x, 32 devices: a whole 2x2x4 slice. The times are simulated.
32 devices in a mesh: ep: 4 (over y, x), tp: 8 (over z, core).
Axes of the slice: x: 2, y: 2, z: 4, core: 2. Of those that a mesh axis runs over, the one named last changes fastest.
Arguments:
- resid: bfloat16 [512, 2048], P('ep'), may hold values from -6 to 6
- norm1_gain: float32 [2048], replicated, may hold values from 0.1 to 1.9
- w_query: bfloat16 [2048, 2048], P('ep', 'tp'), may hold values from -0.125 to 0.125
- w_key: bfloat16 [2048, 2048], P('ep', 'tp'), may hold values from -0.125 to 0.125
- w_value: bfloat16 [2048, 2048], P('ep', 'tp'), may hold values from -0.125 to 0.125
- w_outgate: bfloat16 [2048, 2048], P('ep', 'tp'), may hold values from -0.125 to 0.125
- w_igate: bfloat16 [2048, 32], replicated, may hold values from -0.125 to 0.125
- w_fgate: bfloat16 [2048, 32], replicated, may hold values from -0.125 to 0.125
- forget_bias: float32 [32], replicated, may hold values from 0 to 4
- head_gain: float32 [2048], P('tp'), may hold values from 0.1 to 1.9
- w_out: bfloat16 [2048, 2048], P('tp'), may hold values from -0.125 to 0.125
- state_matrix: float32 [512, 32, 64, 64], P('ep', 'tp'), may hold values from -4 to 4
- state_norm: float32 [512, 32, 64], P('ep', 'tp'), may hold values from -8 to 8
- state_max: float32 [512, 32], P('ep', 'tp'), may hold values from -1 to 2
- norm2_gain: float32 [2048], replicated, may hold values from 0.1 to 1.9
- group_router: bfloat16 [2048, 4], replicated, may hold values from -0.125 to 0.125
- expert_router: bfloat16 [2048, 8], replicated, may hold values from -0.125 to 0.125
- expert_ids: int32 [512, 2], P('ep'), may hold values from 0 to 7, all different within a row; in each aligned block of 128 rows (0 to 127, 128 to 255, ...) at most 48 rows name the same one
- exp_gate: bfloat16 [8, 2048, 1024], P('ep', None, 'tp'), may hold values from -0.125 to 0.125
- exp_up: bfloat16 [8, 2048, 1024], P('ep', None, 'tp'), may hold values from -0.125 to 0.125
- exp_down: bfloat16 [8, 1024, 2048], P('ep', 'tp'), may hold values from -0.1875 to 0.1875
Outputs:
- mixed: bfloat16 [512, 2048], P('ep', 'tp')
- new_matrix: float32 [512, 32, 64, 64], P('ep', 'tp')
- new_normer: float32 [512, 32, 64], P('ep', 'tp')
- new_max: float32 [512, 32], P('ep', 'tp')
Inputs may be any that keep to these rules, and one draw needn't show every extreme that they name: `expert_ids`: A token's 2 experts differ. Among the 128 tokens of one index of ep (aligned blocks of rows) no expert is named more than 48 times, and in some block one expert is named exactly 48 times.
All inputs are finite; a program needn't handle non-finite values.
Results may differ from a plain program's by a relative error of at most 0.014.
Values may be sent and summed in bfloat16 or wider, within the bound.
A program may use at most 128 MiB of HBM per device.

v0:
```python
import jax
import jax.numpy as jnp
from jax import lax
from jax.sharding import PartitionSpec as P

EPSILON = 1e-06


def rms_scale(values, gain):
    widened = values.astype(jnp.float32)
    factor = lax.rsqrt(jnp.mean(widened * widened, axis=-1, keepdims=True) + EPSILON)
    return widened * factor * gain


def memory_cell(scaled, key_rows, value_rows, in_gate, log_forget, matrix, normer, running):
    stable = jnp.maximum(log_forget + running, in_gate)
    fresh = jnp.exp(in_gate - stable)
    carried = jnp.exp(log_forget + running - stable)
    readout = jnp.einsum("bhd,bhde->bhe", scaled, matrix, precision=lax.Precision.HIGHEST)
    score = jnp.sum(scaled * key_rows, axis=-1) * fresh
    numer = carried[..., None] * readout + score[..., None] * value_rows
    denom = carried * jnp.sum(scaled * normer, axis=-1) + score
    cell_out = numer / jnp.maximum(jnp.abs(denom), 1.0)[..., None]
    new_matrix = (
        carried[..., None, None] * matrix
        + fresh[..., None, None] * key_rows[..., :, None] * value_rows[..., None, :]
    )
    new_normer = carried[..., None] * normer + fresh[..., None] * key_rows
    return (cell_out, new_matrix, new_normer, stable)


def per_device(
    resid,
    norm1_gain,
    w_query,
    w_key,
    w_value,
    w_outgate,
    w_igate,
    w_fgate,
    forget_bias,
    head_gain,
    w_out,
    state_matrix,
    state_norm,
    state_max,
    norm2_gain,
    group_router,
    expert_router,
    expert_ids,
    exp_gate,
    exp_up,
    exp_down,
):
    rows = resid.shape[0]
    local_heads = state_matrix.shape[1]
    size = state_matrix.shape[2]
    head_rank = lax.axis_index("tp")
    normed = rms_scale(resid, norm1_gain).astype(jnp.bfloat16)
    features = lax.all_to_all(normed, "ep", split_axis=1, concat_axis=0, tiled=True)
    joined = jnp.concatenate((w_query, w_key, w_value, w_outgate), axis=1)
    projected = lax.psum_scatter(
        jnp.dot(features, joined, preferred_element_type=jnp.float32),
        "ep",
        scatter_dimension=0,
        tiled=True,
    )
    stored = lax.optimization_barrier(projected.astype(jnp.bfloat16)).astype(jnp.float32)
    pieces = jnp.split(stored, 4, axis=1)
    scaled = pieces[0].reshape(rows, local_heads, size) * size ** (-0.5)
    key_rows = pieces[1].reshape(rows, local_heads, size)
    value_rows = pieces[2].reshape(rows, local_heads, size)
    outgate = pieces[3].reshape(rows, local_heads, size)
    head_start = head_rank * local_heads
    gate_cols = lax.dynamic_slice_in_dim(w_igate, head_start, local_heads, 1)
    forget_cols = lax.dynamic_slice_in_dim(w_fgate, head_start, local_heads, 1)
    bias_slice = lax.dynamic_slice_in_dim(forget_bias, head_start, local_heads, 0)
    in_gate = jnp.dot(normed, gate_cols, preferred_element_type=jnp.float32)
    log_forget = jax.nn.log_sigmoid(
        jnp.dot(normed, forget_cols, preferred_element_type=jnp.float32) + bias_slice
    )
    cell_out, new_matrix, new_normer, new_max = memory_cell(
        scaled, key_rows, value_rows, in_gate, log_forget, state_matrix, state_norm, state_max
    )
    headed = cell_out * lax.rsqrt(jnp.mean(cell_out * cell_out, axis=-1, keepdims=True) + EPSILON)
    headed = headed * head_gain.reshape(local_heads, size) * jax.nn.sigmoid(outgate)
    head_out = headed.astype(jnp.bfloat16).reshape(rows, local_heads * size)
    partial_mix = jnp.dot(head_out, w_out, preferred_element_type=jnp.float32)
    attended = lax.psum_scatter(
        partial_mix.astype(jnp.bfloat16), "tp", scatter_dimension=1, tiled=True
    ).astype(jnp.float32)
    column_count = attended.shape[1]
    own_cols = lax.dynamic_slice_in_dim(resid, head_rank * column_count, column_count, 1)
    after_cols = (own_cols.astype(jnp.float32) + attended).astype(jnp.bfloat16)
    after_mix = lax.all_gather(after_cols, "tp", axis=1, tiled=True)
    normed2 = rms_scale(after_mix, norm2_gain).astype(jnp.bfloat16)
    experts_all = expert_router.shape[1]
    groups = group_router.shape[1]
    per_group = experts_all // groups
    topk = expert_ids.shape[1]
    group_exp = jnp.exp(jnp.dot(normed2, group_router, preferred_element_type=jnp.float32))
    group_prob = group_exp / jnp.sum(group_exp, axis=1, keepdims=True)
    expert_logits = jnp.dot(normed2, expert_router, preferred_element_type=jnp.float32)
    expert_range = jnp.arange(experts_all, dtype=jnp.int32)
    one_hot = (expert_ids[:, :, None] == expert_range).astype(jnp.float32)
    chosen_exp = jnp.exp(jnp.sum(one_hot * expert_logits[:, None, :], axis=2))
    share = chosen_exp / jnp.sum(chosen_exp, axis=1, keepdims=True)
    group_hot = (
        (expert_ids // per_group)[:, :, None] == jnp.arange(groups, dtype=jnp.int32)
    ).astype(jnp.float32)
    group_weight = jnp.sum(group_hot * group_prob[:, None, :], axis=2)
    route_weight = group_weight * share
    capacity = max(2, 3 * rows * topk // (2 * experts_all))
    flat_hot = one_hot.reshape(rows * topk, experts_all)
    earlier = jnp.cumsum(flat_hot, axis=0) - flat_hot
    slot = jnp.sum(earlier * flat_hot, axis=1).astype(jnp.int32).reshape(rows, topk)
    position = expert_ids * capacity + slot
    slot_range = jnp.arange(experts_all * capacity, dtype=jnp.int32)
    matched = position[:, :, None] == slot_range
    dispatch = jnp.any(matched, axis=1).astype(jnp.bfloat16)
    combine = jnp.sum(matched.astype(jnp.float32) * route_weight[:, :, None], axis=1)
    buffer = jnp.einsum("ts,td->sd", dispatch, normed2, preferred_element_type=jnp.float32).astype(
        jnp.bfloat16
    )
    ep_count = lax.axis_size("ep")
    local_experts = exp_gate.shape[0]
    buffer = buffer.reshape(ep_count, local_experts, capacity, normed2.shape[1])
    arrived = lax.all_to_all(buffer, "ep", split_axis=0, concat_axis=0, tiled=True)
    gate_part = jnp.einsum("secd,edf->secf", arrived, exp_gate, preferred_element_type=jnp.float32)
    up_part = jnp.einsum("secd,edf->secf", arrived, exp_up, preferred_element_type=jnp.float32)
    units = (jax.nn.silu(gate_part) * up_part).astype(jnp.bfloat16)
    expert_terms = jnp.einsum("secf,efd->secd", units, exp_down, preferred_element_type=jnp.float32)
    summed = lax.psum_scatter(
        expert_terms.astype(jnp.bfloat16), "tp", scatter_dimension=3, tiled=True
    ).astype(jnp.float32)
    returned = lax.all_to_all(
        summed.astype(jnp.bfloat16), "ep", split_axis=0, concat_axis=0, tiled=True
    ).astype(summed.dtype)
    moe = jnp.dot(
        combine,
        returned.reshape(experts_all * capacity, -1),
        precision=lax.Precision.HIGHEST,
        preferred_element_type=jnp.float32,
    )
    mixed = (after_cols.astype(jnp.float32) + moe).astype(jnp.bfloat16)
    return (mixed, new_matrix, new_normer, new_max)


def solution(mesh):
    in_specs = (
        P("ep", None),
        P(),
        P("ep", "tp"),
        P("ep", "tp"),
        P("ep", "tp"),
        P("ep", "tp"),
        P(),
        P(),
        P(),
        P("tp"),
        P("tp", None),
        P("ep", "tp", None, None),
        P("ep", "tp", None),
        P("ep", "tp"),
        P(),
        P(),
        P(),
        P("ep", None),
        P("ep", None, "tp"),
        P("ep", None, "tp"),
        P("ep", "tp", None),
    )
    out_specs = (P("ep", "tp"), P("ep", "tp", None, None), P("ep", "tp", None), P("ep", "tp"))
    return jax.shard_map(
        per_device, mesh=mesh, in_specs=in_specs, out_specs=out_specs, check_vma=False
    )
```

profile of v0, /device:TPU:0, one launch (start us, length us, event | category | flops | bytes accessed | tf_op | source)
XLA Modules:
  0.0 198.8 jit_solution(3308358261850177217)
XLA Ops:
  7.2 1.4 copy.97
  8.7 0.3 fusion.21
  9.0 1.0 fusion.23
  10.0 13.5 %all_to_all.29 = bf16[128,4,512]{0,2,1:T(8,128)(2,1)S(1)} all-to-all(bf16[128,4,512]{0,2,1:T(8,128)(2,1)S(1)} %bitcast.63), channel_id=1, replica_groups=mesh['ep'=4,'tp'=8] {'ep'}, dimensions={1} | all-to-all | bytes 1048576 | tf_op jit(solution)/shard_map/all_to_all | solution.py:60
  23.5 0.2 copy.98
  23.8 3.0 %fusion.27 = f32[512,1024]{1,0:T(8,128)} fusion(bf16[512,512]{1,0:T(8,128)(2,1)S(1)} %bitcast.70, bf16[512,256]{1,0:T(8,128)(2,1)S(1)} %copy-done.8, bf16[512,256]{1,0:T(8,128)(2,1)S(1)} %copy-done.9, bf16[512,256]{1,0:T(8,128)(2,1)S(1)} %copy-done.10, bf16[512,256]{1,0:T(8,128)(2,1)} %param.23), kind=kOutput, calls=%fused_computation.29 | convolution fusion | flops 541065216 | bytes 3670016 | tf_op jit(solution)/shard_map/dot_general | solution.py:63
  26.8 0.0 reduce-scatter.6.cloned.1.call-start
  26.8 0.6 copy-done.6
  27.4 0.1 mul.217
  27.5 0.1 dynamic_slice.14
  27.6 1.0 fusion.49
  28.5 33.3 %reduce-scatter.4.cloned.1.call-done = f32[128,1024]{1,0:T(8,128)} async-done(((f32[512,1024]{1,0:T(8,128)}), f32[128,1024]{1,0:T(8,128)}) %reduce-scatter.4.cloned.1.call-update) | async-done | bytes 524304 | tf_op jit(solution)/shard_map/reduce_scatter | solution.py:62
  61.8 1.1 convert_element_type.75
  63.0 0.1 copy.101
  63.1 0.1 copy.100
  63.2 0.1 copy.99
  63.3 0.1 copy.102
  63.5 1.6 abs_maximum_fusion
  65.0 0.7 multiply_add_fusion.1
  65.7 6.7 %multiply_add_fusion = (f32[128,4,64,64]{0,3,2,1:T(8,128)}, f32[128,4,64]{0,2,1:T(8,128)S(1)}) fusion(f32[128,4,64,64]{0,3,2,1:T(8,128)} %param.32, f32[128,4,64]{0,2,1:T(8,128)S(1)} %bitcast.65, f32[128,4,64]{0,2,1:T(8,128)S(1)} %get-tuple-element.7, f32[128,4]{0,1:T(4,128)S(1)} %get-tuple-element.9, f32[128,4,64]{0,2,1:T(8,128)S(1)} %bitcast.67), kind=kLoop, calls=%fused_computation.1 | loop fusion | flops 10452992 | bytes 17303552 | tf_op jit(solution)/shard_map/add | solution.py:25
  72.5 0.1 multiply_convert_fusion
  72.6 1.1 convolution_convert_fusion.2
  73.8 0.1 copy.103
  74.0 0.1 eq.62
  74.1 0.1 eq.58
  74.2 0.6 reduce-window.6
  74.8 0.2 slice_reduce_fusion
  75.0 0.1 fusion.53
  75.1 0.1 convert_element_type.85
  75.3 0.1 copy.105
  75.4 0.1 fusion.39
  75.5 29.7 %reduce-scatter.6.cloned.1.call-done = bf16[128,256]{1,0:T(8,128)(2,1)} async-done(((bf16[128,2048]{1,0:T(8,128)(2,1)}), bf16[128,256]{1,0:T(8,128)(2,1)}) %reduce-scatter.6.cloned.1.call-update) | async-done | bytes 65552 | tf_op jit(solution)/shard_map/reduce_scatter | solution.py:89
  105.2 0.9 add_convert_fusion
  106.1 14.9 %all_gather.3 = bf16[128,2048]{1,0:T(8,128)(2,1)S(1)} all-gather(bf16[128,256]{1,0:T(8,128)(2,1)S(1)} %add_convert_fusion), channel_id=1, replica_groups=mesh['ep'=4,'tp'=8] {'tp'}, dimensions={1}, use_global_device_ids=true | all-gather | bytes 589824 | tf_op jit(solution)/shard_map/all_gather | solution.py:95
  121.1 0.2 fusion.24
  121.3 0.7 convolution_convert_fusion.1
  122.0 23.8 %all_to_all.30 = bf16[4,2,48,2048]{3,2,1,0:T(8,128)(2,1)S(1)} all-to-all(bf16[4,2,48,2048]{3,2,1,0:T(8,128)(2,1)S(1)} %bitcast.64), channel_id=1, replica_groups=mesh['ep'=4,'tp'=8] {'ep'}, dimensions={0} | all-to-all | bytes 3145728 | tf_op jit(solution)/shard_map/all_to_all | solution.py:128
  145.7 0.6 fusion.5
  146.3 3.4 %fusion = bf16[4,2,48,2048]{3,2,0,1:T(8,128)(2,1)} fusion(bf16[4,2,48,2048]{3,2,1,0:T(8,128)(2,1)S(1)} %all_to_all.30, bf16[2,128,2048]{2,1,0:T(8,128)(2,1)S(1)} %copy-done, bf16[2,2048,128]{2,1,0:T(8,128)(2,1)} %param.40, f32[4,2,48,128]{3,2,0,1:T(8,128)S(1)} %fusion.5), kind=kOutput, calls=%fused_computation.4 | convolution fusion | flops 403734528 | bytes 5439488 | tf_op jit(solution)/shard_map/secf,efd->secd/dot_general | solution.py:132
  149.7 0.3 fusion.64
  150.1 0.3 copy-done.12
  150.4 0.3 fusion.68
  150.8 30.0 %reduce-scatter.8.cloned.1.call-done = bf16[4,2,48,256]{3,2,0,1:T(8,128)(2,1)} async-done(((bf16[4,2,48,2048]{3,2,0,1:T(8,128)(2,1)}), bf16[4,2,48,256]{3,2,0,1:T(8,128)(2,1)}) %reduce-scatter.8.cloned.1.call-update) | async-done | bytes 196624 | tf_op jit(solution)/shard_map/reduce_scatter | solution.py:133
  180.8 1.6 copy.108
  182.4 3.8 %all-to-all-start.2 = ((bf16[4,2,48,256]{3,2,1,0:T(8,128)(2,1)}), bf16[4,2,48,256]{3,2,1,0:T(8,128)(2,1)S(1)}, u32[]{:S(2)}, u32[]{:S(2)}) async-start(bf16[4,2,48,256]{3,2,1,0:T(8,128)(2,1)} %copy.108), calls=%async_computation.5 | async-start | bytes 393216 | tf_op jit(solution)/shard_map/all_to_all | solution.py:136
  186.2 0.1 select_reduce_fusion
  186.4 5.0 %all-to-all-done.2 = bf16[4,2,48,256]{3,2,1,0:T(8,128)(2,1)S(1)} async-done(((bf16[4,2,48,256]{3,2,1,0:T(8,128)(2,1)}), bf16[4,2,48,256]{3,2,1,0:T(8,128)(2,1)S(1)}, u32[]{:S(2)}, u32[]{:S(2)}) %all-to-all-start.2) | async-done | bytes 196640 | tf_op jit(solution)/shard_map/all_to_all | solution.py:136
  191.4 0.9 fusion.19
  (49 shorter events, 0.6 us)
Async XLA Ops:
  7.2 139.1 %copy-start = (bf16[2,128,2048]{2,1,0:T(8,128)(2,1)S(1)}, bf16[2,128,2048]{2,1,0:T(8,128)(2,1)}, u32[]{:S(2)}) copy-start(bf16[2,128,2048]{2,1,0:T(8,128)(2,1)} %param.41) | copy-start | bytes 3145732
  7.2 54.6 %reduce-scatter.4.cloned.1.call-start = ((), (), s32[]{:S(2)}) async-start(), calls=%async_computation.6 | async-start | bytes 2621440 | tf_op jit(solution)/shard_map/reduce_scatter | solution.py:62
  8.6 15.1 %copy-start.8 = (bf16[512,256]{1,0:T(8,128)(2,1)S(1)}, bf16[512,256]{1,0:T(8,128)(2,1)}, u32[]{:S(2)}) copy-start(bf16[512,256]{1,0:T(8,128)(2,1)} %param.26) | copy-start | bytes 786436
  8.6 15.1 %copy-start.9 = (bf16[512,256]{1,0:T(8,128)(2,1)S(1)}, bf16[512,256]{1,0:T(8,128)(2,1)}, u32[]{:S(2)}) copy-start(bf16[512,256]{1,0:T(8,128)(2,1)} %param.25) | copy-start | bytes 786436
  8.6 15.1 %copy-start.10 = (bf16[512,256]{1,0:T(8,128)(2,1)S(1)}, bf16[512,256]{1,0:T(8,128)(2,1)}, u32[]{:S(2)}) copy-start(bf16[512,256]{1,0:T(8,128)(2,1)} %param.24) | copy-start | bytes 786436
  26.7 0.7 copy-start.6
  26.7 0.8 copy-start.13
  26.8 78.5 %reduce-scatter.6.cloned.1.call-start = ((), (), s32[]{:S(2)}) async-start(), calls=%async_computation.7 | async-start | bytes 589824 | tf_op jit(solution)/shard_map/reduce_scatter | solution.py:89
  27.6 35.9 %copy-start.2 = (f32[128,4,64]{0,2,1:T(8,128)S(1)}, f32[128,4,64]{0,2,1:T(8,128)}, u32[]{:S(2)}) copy-start(f32[128,4,64]{0,2,1:T(8,128)} %param.33) | copy-start | bytes 393220
  28.5 34.9 %copy-start.5 = (f32[128,4]{0,1:T(4,128)S(1)}, f32[128,4]{0,1:T(4,128)}, u32[]{:S(2)}) copy-start(f32[128,4]{0,1:T(4,128)} %param.34) | copy-start | bytes 6148
  65.7 6.9 %copy-start.1 = (bf16[256,2048]{1,0:T(8,128)(2,1)S(1)}, bf16[256,2048]{1,0:T(8,128)(2,1)}, u32[]{:S(2)}) copy-start(bf16[256,2048]{1,0:T(8,128)(2,1)} %param.31) | copy-start | bytes 3145732
  72.4 1.4 copy-start.3
  72.5 48.8 %copy-start.4 = (f32[2048]{0:T(1024)S(1)}, f32[2048]{0:T(1024)}, u32[]{:S(2)}) copy-start(f32[2048]{0:T(1024)} %param.35) | copy-start | bytes 24580
  73.8 107.0 %reduce-scatter.8.cloned.1.call-start = ((), (), s32[]{:S(2)}) async-start(), calls=%async_computation.8 | async-start | bytes 1769472 | tf_op jit(solution)/shard_map/reduce_scatter | solution.py:133
  121.9 23.8 %copy-start.7 = (bf16[2,2048,128]{2,1,0:T(8,128)(2,1)S(1)}, bf16[2,2048,128]{2,1,0:T(8,128)(2,1)}, u32[]{:S(2)}) copy-start(bf16[2,2048,128]{2,1,0:T(8,128)(2,1)} %param.39) | copy-start | bytes 3145732
  146.3 3.4 %copy-start.11 = (bf16[2048,8]{0,1:T(8,128)(2,1)S(1)}, bf16[2048,8]{0,1:T(8,128)(2,1)}, u32[]{:S(2)}) copy-start(bf16[2048,8]{0,1:T(8,128)(2,1)} %param.37) | copy-start | bytes 98308
  149.7 0.7 copy-start.12
  182.4 9.0 %all-to-all-start.2 = ((bf16[4,2,48,256]{3,2,1,0:T(8,128)(2,1)}), bf16[4,2,48,256]{3,2,1,0:T(8,128)(2,1)S(1)}, u32[]{:S(2)}, u32[]{:S(2)}) async-start(bf16[4,2,48,256]{3,2,1,0:T(8,128)(2,1)} %copy.108), calls=%async_computation.5 | async-start | bytes 393216 | tf_op jit(solution)/shard_map/all_to_all | solution.py:136
Sparse Core Ops, SparseCore 0:
  26.9 34.8 reduce-scatter.3
  73.9 31.2 reduce-scatter.5
  149.8 30.9 reduce-scatter.7
where the time goes:
time: 199 us
  waiting for transfers between devices  98.1 us (49%)
  blocking collectives  52.2 us (26%)
  between operations  14.1 us (7%)
  matrix products  12.7 us (6%)
  other arithmetic  12.2 us (6%)
  local copies, waits for them, and re-layouts  5.48 us (3%)
  starting transfers between devices  3.93 us (2%)
    reduce_scatter x1, waiting for transfers between devices, per_device(): lax.psum_scatter(jnp.dot(features, joined, preferred_element_type=jnp.flo...  33.3 us
    reduce_scatter x1, waiting for transfers between devices, per_device(): lax.psum_scatter(expert_terms.astype(jnp.bfloat16), 'tp', scatter_dimensi...  30 us
    reduce_scatter x1, waiting for transfers between devices, per_device(): lax.psum_scatter(partial_mix.astype(jnp.bfloat16), 'tp', scatter_dimensio...  29.7 us
    all_to_all x1, blocking collectives, per_device(): lax.all_to_all(buffer, 'ep', split_axis=0, concat_axis=0, tiled=True)  23.8 us
    all_gather x1, blocking collectives, per_device(): after_mix = lax.all_gather(after_cols, 'tp', axis=1, tiled=True)  14.9 us
    all_to_all x1, blocking collectives, per_device(): lax.all_to_all(normed, 'ep', split_axis=1, concat_axis=0, tiled=True)  13.5 us
    add x1, other arithmetic, memory_cell(): carried[..., None, None] * matrix  6.72 us
    all_to_all x1, waiting for transfers between devices, per_device(): lax.all_to_all(summed.astype(jnp.bfloat16), 'ep', split_axis=0, concat_ax...  5.04 us
  transfers between devices with their start and end apart: 4, of which 4 were waited for; matrix products, arithmetic and copies ran while one was open for 2% of the time, Pallas kernels for 0%

commit v1 on v0

v1 whole, which is shorter than its diff:
```python
import functools

import jax
import jax.numpy as jnp
from jax import lax
from jax.experimental import pallas as pl
from jax.experimental.pallas import tpu as pltpu
from jax.sharding import PartitionSpec as P

EPSILON = 1e-06


def rms_scale(values, gain):
    widened = values.astype(jnp.float32)
    factor = lax.rsqrt(jnp.mean(widened * widened, axis=-1, keepdims=True) + EPSILON)
    return widened * factor * gain


def memory_cell(scaled, key_rows, value_rows, in_gate, log_forget, matrix, normer, running):
    stable = jnp.maximum(log_forget + running, in_gate)
    fresh = jnp.exp(in_gate - stable)
    carried = jnp.exp(log_forget + running - stable)
    readout = jnp.einsum("bhd,bhde->bhe", scaled, matrix, precision=lax.Precision.HIGHEST)
    score = jnp.sum(scaled * key_rows, axis=-1) * fresh
    numer = carried[..., None] * readout + score[..., None] * value_rows
    denom = carried * jnp.sum(scaled * normer, axis=-1) + score
    cell_out = numer / jnp.maximum(jnp.abs(denom), 1.0)[..., None]
    new_matrix = (
        carried[..., None, None] * matrix
        + fresh[..., None, None] * key_rows[..., :, None] * value_rows[..., None, :]
    )
    new_normer = carried[..., None] * normer + fresh[..., None] * key_rows
    return (cell_out, new_matrix, new_normer, stable)


MESH = pl.DeviceIdType.MESH
VMEM = pl.BlockSpec(memory_space=pltpu.VMEM)
ANY = pl.BlockSpec(memory_space=pl.ANY)


def remote(src, dst, send_sem, recv_sem, device):
    return pltpu.make_async_remote_copy(
        src_ref=src,
        dst_ref=dst,
        send_sem=send_sem,
        recv_sem=recv_sem,
        device_id=device,
        device_id_type=MESH,
    )


def greet(devices):
    barrier = pltpu.get_barrier_semaphore()
    for device in devices:
        pl.semaphore_signal(barrier, inc=1, device_id=device, device_id_type=MESH)


def project_kernel(
    n, resid, gain, wq, wk, wv, wo, wi, wf, out, in_gate, forget,
    blocks, arrived, sent, returned, weights, total, wsem, fs, fr, rs, rr,
):
    me = lax.axis_index("ep")
    ahead = [lax.rem(me + k, n) for k in range(n)]
    behind = [lax.rem(me + n - k, n) for k in range(n)]
    greet([{"ep": ahead[k]} for k in range(1, n)])
    width = wq.shape[1]
    depth = wq.shape[0]
    loads = []
    for i, w in enumerate((wq, wk, wv, wo)):
        load = pltpu.make_async_copy(w, weights.at[:, i * width : (i + 1) * width], wsem.at[i])
        load.start()
        loads.append(load)
    normed = rms_scale(resid[...], gain[...]).astype(jnp.bfloat16)
    for j in range(n):
        blocks[j] = normed[:, j * depth : (j + 1) * depth]
    pl.semaphore_wait(pltpu.get_barrier_semaphore(), n - 1)
    forward = {}
    for k in range(1, n):
        forward[k] = remote(blocks.at[ahead[k]], arrived.at[k], fs.at[k], fr.at[k], {"ep": ahead[k]})
        forward[k].start()
    in_gate[...] = jnp.dot(normed, wi[...], preferred_element_type=jnp.float32)
    forget[...] = jnp.dot(normed, wf[...], preferred_element_type=jnp.float32)
    for load in loads:
        load.wait()
    total[...] = jnp.dot(blocks[me], weights[...], preferred_element_type=jnp.float32)
    back = {}
    for k in range(1, n):
        forward[k].wait_recv()
        sent[k] = jnp.dot(arrived[k], weights[...], preferred_element_type=jnp.float32).astype(
            jnp.bfloat16
        )
        back[k] = remote(sent.at[k], returned.at[k], rs.at[k], rr.at[k], {"ep": behind[k]})
        back[k].start()
    for k in range(1, n):
        back[k].wait_recv()
        total[...] += returned[k].astype(jnp.float32)
    out[...] = total[...].astype(jnp.bfloat16)
    for k in range(1, n):
        forward[k].wait_send()
        back[k].wait_send()


def project(resid, gain, wq, wk, wv, wo, wi, wf):
    n = lax.axis_size("ep")
    rows = resid.shape[0]
    depth, width = wq.shape
    dma = pltpu.SemaphoreType.DMA
    bf16, f32 = jnp.bfloat16, jnp.float32
    return pl.pallas_call(
        functools.partial(project_kernel, n),
        out_shape=(
            jax.ShapeDtypeStruct((rows, 4 * width), bf16),
            jax.ShapeDtypeStruct((rows, wi.shape[1]), f32),
            jax.ShapeDtypeStruct((rows, wi.shape[1]), f32),
        ),
        in_specs=[VMEM, VMEM, ANY, ANY, ANY, ANY, VMEM, VMEM],
        out_specs=(VMEM, VMEM, VMEM),
        scratch_shapes=[
            pltpu.VMEM((n, rows, depth), bf16),
            pltpu.VMEM((n, rows, depth), bf16),
            pltpu.VMEM((n, rows, 4 * width), bf16),
            pltpu.VMEM((n, rows, 4 * width), bf16),
            pltpu.VMEM((depth, 4 * width), bf16),
            pltpu.VMEM((rows, 4 * width), f32),
            dma((4,)), dma((n,)), dma((n,)), dma((n,)), dma((n,)),
        ],
        compiler_params=pltpu.CompilerParams(
            collective_id=0, has_side_effects=True, vmem_limit_bytes=32 * 1024 * 1024
        ),
    )(resid, gain.reshape(1, -1), wq, wk, wv, wo, wi, wf)


def mix_kernel(
    nt, head, w, own_cols, after_out, full_out,
    full, pair_s, pair_r, red_s, red_r, gathered, ps, pr, rs, rr, gs, gr, os, orr,
):
    t = lax.axis_index("tp")
    nz = nt // 2
    z, c = t // 2, lax.rem(t, 2)
    partner = {"tp": t + 1 - 2 * c}
    ahead = [lax.rem(z + k, nz) for k in range(nz)]
    behind = [lax.rem(z + nz - k, nz) for k in range(nz)]
    peers = [{"tp": 2 * ahead[k] + c} for k in range(nz)]
    greet([partner] + peers[1:])
    cols = own_cols.shape[1]
    full[...] = jnp.dot(head[...], w[...], preferred_element_type=jnp.float32)

    def block(dest):
        return full[:, pl.ds(pl.multiple_of(dest * cols, cols), cols)]

    for k in range(nz):
        pair_s[k] = block(2 * ahead[k] + 1 - c).astype(jnp.bfloat16)
    pl.semaphore_wait(pltpu.get_barrier_semaphore(), nz)
    order = list(range(1, nz)) + [0]
    pair = {}
    for k in order:
        pair[k] = remote(pair_s.at[k], pair_r.at[k], ps.at[k], pr.at[k], partner)
        pair[k].start()
    reduce = {}
    for k in order:
        pair[k].wait_recv()
        value = block(2 * ahead[k] + c) + pair_r[k].astype(jnp.float32)
        if k == 0:
            total = value
        else:
            red_s[k] = value.astype(jnp.bfloat16)
            reduce[k] = remote(red_s.at[k], red_r.at[k], rs.at[k], rr.at[k], peers[k])
            reduce[k].start()
    for k in range(1, nz):
        reduce[k].wait_recv()
        total = total + red_r[k].astype(jnp.float32)
    after = (own_cols[...].astype(jnp.float32) + total).astype(jnp.bfloat16)
    after_out[...] = after
    gathered[t] = after
    gather, over = {}, {}
    for k in range(1, nz):
        gather[k] = remote(gathered.at[t], gathered.at[t], gs.at[k], gr.at[k], peers[k])
        gather[k].start()
    for k in range(nz):
        origin = 2 * behind[k] + c
        if k > 0:
            gather[k].wait_recv()
        over[k] = remote(gathered.at[origin], gathered.at[origin], os.at[k], orr.at[k], partner)
        over[k].start()
    for k in range(nz):
        over[k].wait_recv()
    for j in range(nt):
        full_out[:, j * cols : (j + 1) * cols] = gathered[j]
    for k in range(nz):
        pair[k].wait_send()
        over[k].wait_send()
        if k > 0:
            reduce[k].wait_send()
            gather[k].wait_send()


def mix(head, w, own_cols):
    nt = lax.axis_size("tp")
    nz = nt // 2
    rows, cols = own_cols.shape
    dma = pltpu.SemaphoreType.DMA
    bf16, f32 = jnp.bfloat16, jnp.float32
    return pl.pallas_call(
        functools.partial(mix_kernel, nt),
        out_shape=(
            jax.ShapeDtypeStruct((rows, cols), bf16),
            jax.ShapeDtypeStruct((rows, cols * nt), bf16),
        ),
        in_specs=[VMEM, VMEM, VMEM],
        out_specs=(VMEM, VMEM),
        scratch_shapes=[
            pltpu.VMEM((rows, cols * nt), f32),
            pltpu.VMEM((nz, rows, cols), bf16),
            pltpu.VMEM((nz, rows, cols), bf16),
            pltpu.VMEM((nz, rows, cols), bf16),
            pltpu.VMEM((nz, rows, cols), bf16),
            pltpu.VMEM((nt, rows, cols), bf16),
        ]
        + [dma((nz,))] * 8,
        compiler_params=pltpu.CompilerParams(
            collective_id=1, has_side_effects=True, vmem_limit_bytes=32 * 1024 * 1024
        ),
    )(head, w, own_cols)


def expert_kernel(
    n, nt, disp, comb, wg, wu, wd, out,
    arr, vg, vu, vd, full, pair_s, pair_r, ret_s, ret_r, z_s, z_r,
    wsem, ds, dr, fs, fr, ps, pr, rs, rr, zs, zr,
):
    me = lax.axis_index("ep")
    t = lax.axis_index("tp")
    nz = nt // 2
    z, c = t // 2, lax.rem(t, 2)
    partner = {"tp": t + 1 - 2 * c}
    ahead = [lax.rem(me + k, n) for k in range(n)]
    behind = [lax.rem(me + n - k, n) for k in range(n)]
    z_ahead = [lax.rem(z + k, nz) for k in range(nz)]
    z_peers = [{"tp": 2 * z_ahead[k] + c} for k in range(nz)]
    greet([{"ep": ahead[k]} for k in range(1, n)] + [partner] + z_peers[1:])
    loads = []
    for i, (w, v) in enumerate(((wg, vg), (wu, vu), (wd, vd))):
        load = pltpu.make_async_copy(w, v, wsem.at[i])
        load.start()
        loads.append(load)
    half = arr.shape[3]
    local = vg.shape[0]
    cap = disp.shape[1] // local
    cols = out.shape[1]
    pl.semaphore_wait(pltpu.get_barrier_semaphore(), n - 1 + nz)
    mine = pl.ds(pl.multiple_of(c * half, half), half)
    send, pass_on, pair, ret = {}, {}, {}, {}
    for k in range(1, n):
        send[k] = remote(
            disp.at[ahead[k], :, mine], arr.at[c, k], ds.at[k], dr.at[k], {"ep": ahead[k]}
        )
        send[k].start()
    arr[0, 0] = disp[me, :, :half]
    arr[1, 0] = disp[me, :, half:]
    for load in loads:
        load.wait()

    def block(k, dest):
        return full[k, :, pl.ds(pl.multiple_of(dest * cols, cols), cols)]

    def compute(k):
        for e in range(local):
            lines = slice(e * cap, (e + 1) * cap)
            low, high = arr[0, k, lines, :], arr[1, k, lines, :]

            def both(v):
                return jnp.dot(
                    low, v[e, :half, :], preferred_element_type=jnp.float32
                ) + jnp.dot(high, v[e, half:, :], preferred_element_type=jnp.float32)

            units = (jax.nn.silu(both(vg)) * both(vu)).astype(jnp.bfloat16)
            full[k, lines, :] = jnp.dot(units, vd[e], preferred_element_type=jnp.float32)
        for i in range(nz):
            pair_s[k, i] = block(k, 2 * i + 1 - c).astype(jnp.bfloat16)
        pair[k] = remote(pair_s.at[k], pair_r.at[k], ps.at[k], pr.at[k], partner)
        pair[k].start()

    def reply(k):
        pair[k].wait_recv()
        for i in range(nz):
            ret_s[k, i] = (block(k, 2 * i + c) + pair_r[k, i].astype(jnp.float32)).astype(
                jnp.bfloat16
            )
        if k > 0:
            ret[k] = remote(ret_s.at[k], ret_r.at[k], rs.at[k], rr.at[k], {"ep": behind[k]})
            ret[k].start()

    compute(0)
    for k in range(1, n):
        send[k].wait_recv()
        pass_on[k] = remote(arr.at[c, k], arr.at[c, k], fs.at[k], fr.at[k], partner)
        pass_on[k].start()
        pass_on[k].wait_recv()
        compute(k)
        reply(k)
    reply(0)
    ret_r[0] = ret_s[0]
    weights = []
    for k in range(n):
        exact = comb[ahead[k]]
        coarse = exact.astype(jnp.bfloat16)
        weights.append((coarse, (exact - coarse.astype(jnp.float32)).astype(jnp.bfloat16)))
        if k > 0:
            ret[k].wait_recv()
    gather = {}
    for i in list(range(1, nz)) + [0]:
        total = jnp.zeros(out.shape, jnp.float32)
        for k in range(n):
            part = ret_r[k, z_ahead[i]]
            for weight in weights[k]:
                total = total + jnp.dot(weight, part, preferred_element_type=jnp.float32)
        if i > 0:
            z_s[i] = total.astype(jnp.bfloat16)
            gather[i] = remote(z_s.at[i], z_r.at[i], zs.at[i], zr.at[i], z_peers[i])
            gather[i].start()
    for i in range(1, nz):
        gather[i].wait_recv()
        total = total + z_r[i].astype(jnp.float32)
    out[...] = total
    for k in range(n):
        pair[k].wait_send()
        if k > 0:
            send[k].wait_send()
            pass_on[k].wait_send()
            ret[k].wait_send()
    for i in range(1, nz):
        gather[i].wait_send()


def experts(disp, comb, wg, wu, wd):
    n, nt = lax.axis_size("ep"), lax.axis_size("tp")
    nz = nt // 2
    slots, width = disp.shape[1:]
    rows = comb.shape[1]
    cols = width // nt
    dma = pltpu.SemaphoreType.DMA
    bf16, f32 = jnp.bfloat16, jnp.float32
    return pl.pallas_call(
        functools.partial(expert_kernel, n, nt),
        out_shape=jax.ShapeDtypeStruct((rows, cols), f32),
        in_specs=[VMEM, VMEM, ANY, ANY, ANY],
        out_specs=VMEM,
        scratch_shapes=[
            pltpu.VMEM((2, n, slots, width // 2), bf16),
            pltpu.VMEM(wg.shape, bf16),
            pltpu.VMEM(wu.shape, bf16),
            pltpu.VMEM(wd.shape, bf16),
            pltpu.VMEM((n, slots, width), f32),
            pltpu.VMEM((n, nz, slots, cols), bf16),
            pltpu.VMEM((n, nz, slots, cols), bf16),
            pltpu.VMEM((n, nz, slots, cols), bf16),
            pltpu.VMEM((n, nz, slots, cols), bf16),
            pltpu.VMEM((nz, rows, cols), bf16),
            pltpu.VMEM((nz, rows, cols), bf16),
            dma((3,)),
        ]
        + [dma((n,))] * 8
        + [dma((nz,))] * 2,
        compiler_params=pltpu.CompilerParams(
            collective_id=2, has_side_effects=True, vmem_limit_bytes=48 * 1024 * 1024
        ),
    )(disp, comb, wg, wu, wd)


def per_device(
    resid,
    norm1_gain,
    w_query,
    w_key,
    w_value,
    w_outgate,
    w_igate,
    w_fgate,
    forget_bias,
    head_gain,
    w_out,
    state_matrix,
    state_norm,
    state_max,
    norm2_gain,
    group_router,
    expert_router,
    expert_ids,
    exp_gate,
    exp_up,
    exp_down,
):
    rows = resid.shape[0]
    local_heads = state_matrix.shape[1]
    size = state_matrix.shape[2]
    head_rank = lax.axis_index("tp")
    projected, in_all, forget_all = project(
        resid, norm1_gain, w_query, w_key, w_value, w_outgate, w_igate, w_fgate
    )
    stored = projected.astype(jnp.float32)
    pieces = jnp.split(stored, 4, axis=1)
    scaled = pieces[0].reshape(rows, local_heads, size) * size ** (-0.5)
    key_rows = pieces[1].reshape(rows, local_heads, size)
    value_rows = pieces[2].reshape(rows, local_heads, size)
    outgate = pieces[3].reshape(rows, local_heads, size)
    head_start = head_rank * local_heads
    bias_slice = lax.dynamic_slice_in_dim(forget_bias, head_start, local_heads, 0)
    in_gate = lax.dynamic_slice_in_dim(in_all, head_start, local_heads, 1)
    log_forget = jax.nn.log_sigmoid(
        lax.dynamic_slice_in_dim(forget_all, head_start, local_heads, 1) + bias_slice
    )
    cell_out, new_matrix, new_normer, new_max = memory_cell(
        scaled, key_rows, value_rows, in_gate, log_forget, state_matrix, state_norm, state_max
    )
    headed = cell_out * lax.rsqrt(jnp.mean(cell_out * cell_out, axis=-1, keepdims=True) + EPSILON)
    headed = headed * head_gain.reshape(local_heads, size) * jax.nn.sigmoid(outgate)
    head_out = headed.astype(jnp.bfloat16).reshape(rows, local_heads * size)
    column_count = resid.shape[1] // lax.axis_size("tp")
    own_cols = lax.dynamic_slice_in_dim(resid, head_rank * column_count, column_count, 1)
    after_cols, after_mix = mix(head_out, w_out, own_cols)
    normed2 = rms_scale(after_mix, norm2_gain).astype(jnp.bfloat16)
    experts_all = expert_router.shape[1]
    groups = group_router.shape[1]
    per_group = experts_all // groups
    topk = expert_ids.shape[1]
    group_exp = jnp.exp(jnp.dot(normed2, group_router, preferred_element_type=jnp.float32))
    group_prob = group_exp / jnp.sum(group_exp, axis=1, keepdims=True)
    expert_logits = jnp.dot(normed2, expert_router, preferred_element_type=jnp.float32)
    expert_range = jnp.arange(experts_all, dtype=jnp.int32)
    one_hot = (expert_ids[:, :, None] == expert_range).astype(jnp.float32)
    chosen_exp = jnp.exp(jnp.sum(one_hot * expert_logits[:, None, :], axis=2))
    share = chosen_exp / jnp.sum(chosen_exp, axis=1, keepdims=True)
    group_hot = (
        (expert_ids // per_group)[:, :, None] == jnp.arange(groups, dtype=jnp.int32)
    ).astype(jnp.float32)
    group_weight = jnp.sum(group_hot * group_prob[:, None, :], axis=2)
    route_weight = group_weight * share
    capacity = max(2, 3 * rows * topk // (2 * experts_all))
    capacity = -(-capacity // 16) * 16
    flat_hot = one_hot.reshape(rows * topk, experts_all)
    earlier = jnp.cumsum(flat_hot, axis=0) - flat_hot
    slot = jnp.sum(earlier * flat_hot, axis=1).astype(jnp.int32).reshape(rows, topk)
    position = expert_ids * capacity + slot
    slot_range = jnp.arange(experts_all * capacity, dtype=jnp.int32)
    matched = position[:, :, None] == slot_range
    dispatch = jnp.any(matched, axis=1).astype(jnp.bfloat16)
    ep_count = lax.axis_size("ep")
    spread = matched.astype(jnp.float32) * route_weight[:, :, None]
    combine = jnp.sum(spread, axis=1).reshape(rows, ep_count, -1).transpose(1, 0, 2)
    buffer = jnp.einsum("ts,td->sd", dispatch, normed2, preferred_element_type=jnp.float32).astype(
        jnp.bfloat16
    )
    buffer = buffer.reshape(ep_count, -1, normed2.shape[1])
    moe = experts(buffer, combine, exp_gate, exp_up, exp_down)
    mixed = (after_cols.astype(jnp.float32) + moe).astype(jnp.bfloat16)
    return (mixed, new_matrix, new_normer, new_max)


def solution(mesh):
    in_specs = (
        P("ep", None),
        P(),
        P("ep", "tp"),
        P("ep", "tp"),
        P("ep", "tp"),
        P("ep", "tp"),
        P(),
        P(),
        P(),
        P("tp"),
        P("tp", None),
        P("ep", "tp", None, None),
        P("ep", "tp", None),
        P("ep", "tp"),
        P(),
        P(),
        P(),
        P("ep", None),
        P("ep", None, "tp"),
        P("ep", None, "tp"),
        P("ep", "tp", None),
    )
    out_specs = (P("ep", "tp"), P("ep", "tp", None, None), P("ep", "tp", None), P("ep", "tp"))
    return jax.shard_map(
        per_device, mesh=mesh, in_specs=in_specs, out_specs=out_specs, check_vma=False
    )
```

time: 199 us -> 107 us (0.54)
  waiting for transfers between devices: 98.1 us -> 0 us
  Pallas kernels: 0 us -> 75.5 us
  blocking collectives: 52.2 us -> 0 us
  between operations: 14.1 us -> 0.92 us
  local copies, waits for them, and re-layouts: 5.48 us -> 16.9 us
  matrix products: 12.7 us -> 1.31 us
  starting transfers between devices: 3.93 us -> 0 us
    reduce_scatter x3 -> x0, waiting for transfers between devices: 93.1 us -> none  [the longest x1 33.3 us: per_device(): lax.psum_scatter(jnp.dot(features, joined, preferred_element_type=jnp.flo...]
    pallas_call x0 -> x3, Pallas kernels: none -> 75.5 us  [the longest x1 33.2 us: experts(): pl.pallas_call(functools.partial(expert_kernel, n, nt), out_shape=jax.Sha...]
    all_to_all x2 -> x0, blocking collectives: 37.3 us -> none  [the longest x1 23.8 us: per_device(): lax.all_to_all(buffer, 'ep', split_axis=0, concat_axis=0, tiled=True)]
    all_gather x1 -> x0, blocking collectives: 14.9 us -> none  [per_device(): after_mix = lax.all_gather(after_cols, 'tp', axis=1, tiled=True)]
    dot_general x7 -> x0, matrix products: 11.4 us -> none  [the longest x1 3.35 us: per_device(): jnp.einsum('secf,efd->secd', units, exp_down, preferred_element_type=jnp....]
    unnamed x30 -> x35, local copies, waits for them, and re-layouts: 2.49 us -> 12.6 us
    all_to_all x1 -> x0, waiting for transfers between devices: 5.04 us -> none  [per_device(): lax.all_to_all(summed.astype(jnp.bfloat16), 'ep', split_axis=0, concat_ax...]
    all_to_all x1 -> x0, starting transfers between devices: 3.81 us -> none  [per_device(): lax.all_to_all(summed.astype(jnp.bfloat16), 'ep', split_axis=0, concat_ax...]
  transfers between devices with their start and end apart: 4 -> 0, of which waited for: 4 -> 0; matrix products, arithmetic and copies ran while one was open for 2% -> 0% of each run, Pallas kernels for 0% -> 0%
where the time goes in v1:
time: 107 us; the launch traced here: 106 us
  Pallas kernels  75.5 us (71%)
  local copies, waits for them, and re-layouts  16.9 us (16%)
  other arithmetic  11.4 us (11%)
  matrix products  1.31 us (1%)
    pallas_call x1, Pallas kernels, experts(): pl.pallas_call(functools.partial(expert_kernel, n, nt), out_shape=jax.Sha...  33.2 us
    pallas_call x1, Pallas kernels, project(): pl.pallas_call(functools.partial(project_kernel, n), out_shape=(jax.Shape...  24.7 us
    pallas_call x1, Pallas kernels, mix(): pl.pallas_call(functools.partial(mix_kernel, nt), out_shape=(jax.ShapeDty...  17.7 us
    unnamed x35, local copies, waits for them, and re-layouts  12.6 us
    add x1, other arithmetic, memory_cell(): carried[..., None, None] * matrix  6.78 us

profile of v1, /device:TPU:0, one launch (start us, length us, event | category | flops | bytes accessed | tf_op | source)
XLA Modules:
  0.0 106.1 jit_solution(7297115318096254786)
XLA Ops:
  0.7 0.8 copy.130
  1.5 0.1 eq.62
  1.6 0.6 reduce-window.6
  2.2 0.2 slice_reduce_fusion
  2.4 0.1 eq.58
  2.6 0.1 fusion.10
  2.7 0.1 convert_element_type.45
  2.9 0.7 and_select_fusion
  3.6 0.1 fusion.3
  3.7 1.2 %copy.116.wi = bf16[2048,32]{1,0:T(8,128)(2,1)S(1)} copy(bf16[2048,32]{0,1:T(8,128)(2,1)} %param.27) | data formatting | bytes 262144 | tf_op args[6]
  4.9 1.2 %copy.117.wf = bf16[2048,32]{1,0:T(8,128)(2,1)S(1)} copy(bf16[2048,32]{0,1:T(8,128)(2,1)} %param.28) | data formatting | bytes 262144 | tf_op args[7]
  6.1 1.0 copy-done.5
  7.1 0.9 copy-done.6
  8.1 0.9 copy-done.7
  9.0 0.9 copy-done.8
  10.0 0.9 copy-done.9
  10.9 0.7 copy-done.10
  11.6 24.7 %shard_map.228 = (bf16[128,1024]{1,0:T(8,128)(2,1)S(1)}, f32[128,32]{1,0:T(8,128)S(1)}, f32[128,32]{1,0:T(8,128)S(1)}) custom-call(bf16[128,2048]{1,0:T(8,128)(2,1)S(1)} %copy-done.5, f32[1,2048]{1,0:T(1,128)S(1)} %bitcast.29, bf16[512,256]{1,0:T(8,128)(2,1)S(1)} %copy-done.6, bf16[512,256]{1,0:T(8,128)(2,1)S(1)} %copy-done.7, ...), custom_call_target="tpu_custom_call" | custom-call | tf_op jit(solution)/shard_map/pallas_call | solution.py:109
  36.4 0.1 copy.128
  36.5 0.8 mul.185
  37.3 0.1 copy.121
  37.4 0.1 copy.122
  37.5 0.9 multiply_reduce_fusion.2
  38.4 0.1 copy.126
  38.5 0.8 copy.119
  39.3 0.7 dynamic_slice.13
  40.1 0.1 copy.123
  40.2 0.1 abs_maximum_fusion
  40.5 0.1 copy.125
  40.7 0.1 copy.136
  40.7 0.7 multiply_add_fusion.1
  41.5 6.8 %multiply_add_fusion = (f32[128,4,64,64]{0,3,2,1:T(8,128)}, f32[128,4,64]{0,2,1:T(8,128)S(1)}) fusion(f32[128,4,64,64]{0,3,2,1:T(8,128)} %param.32, f32[128,4,64]{0,2,1:T(8,128)S(1)} %bitcast.30, f32[128,4,64]{0,2,1:T(8,128)S(1)} %get-tuple-element.37, f32[128,4]{0,1:T(4,128)S(1)} %copy.120, f32[128,4,64]{0,2,1:T(8,128)S(1)} %bitcast.31), kind=kLoop, calls=%fused_computation.1 | loop fusion | flops 10452992 | bytes 17303552 | tf_op jit(solution)/shard_map/add | solution.py:29
  48.3 0.1 multiply_convert_fusion
  48.4 0.1 copy.129.head
  48.5 0.8 constant_dynamic-slice_fusion.own_cols
  49.4 17.7 %shard_map.229 = (bf16[128,256]{1,0:T(8,128)(2,1)S(1)}, bf16[128,2048]{1,0:T(8,128)(2,1)S(1)}) custom-call(bf16[128,256]{1,0:T(8,128)(2,1)S(1)} %copy.129.head, bf16[256,2048]{1,0:T(8,128)(2,1)S(1)} %copy-done.4, bf16[128,256]{1,0:T(8,128)(2,1)S(1)} %constant_dynamic-slice_fusion.own_cols), custom_call_target="tpu_custom_call" | custom-call | tf_op jit(solution)/shard_map/pallas_call | solution.py:203
  67.0 0.2 fusion
  67.3 0.7 convolution_convert_fusion
  67.9 0.3 fusion.17
  68.3 0.3 fusion.12
  68.7 0.1 select_reduce_fusion
  68.9 0.1 copy.133
  69.0 0.1 copy.134
  69.1 1.2 %copy-done.2 = bf16[2,2048,128]{2,1,0:T(8,128)(2,1)S(1)} copy-done((bf16[2,2048,128]{2,1,0:T(8,128)(2,1)S(1)}, bf16[2,2048,128]{2,1,0:T(8,128)(2,1)}, u32[]{:S(2)}) %copy-start.2) | copy-done | bytes 1048600
  70.4 1.2 %copy-done.3 = bf16[2,128,2048]{2,1,0:T(8,128)(2,1)S(1)} copy-done((bf16[2,128,2048]{2,1,0:T(8,128)(2,1)S(1)}, bf16[2,128,2048]{2,1,0:T(8,128)(2,1)}, u32[]{:S(2)}) %copy-start.3) | copy-done | bytes 1048600
  71.6 33.2 %shard_map.230 = f32[128,256]{1,0:T(8,128)S(1)} custom-call(bf16[4,96,2048]{2,1,0:T(8,128)(2,1)S(1)} %bitcast.27, f32[4,128,96]{2,1,0:T(8,128)S(1)} %bitcast.28, bf16[2,2048,128]{2,1,0:T(8,128)(2,1)S(1)} %copy-done.1, bf16[2,2048,128]{2,1,0:T(8,128)(2,1)S(1)} %copy-done.2, bf16[2,128,2048]{2,1,0:T(8,128)(2,1)S(1)} %copy-done.3), custom_call_target="tpu_custom_call" | custom-call | tf_op jit(solution)/shard_map/pallas_call | solution.py:343
  104.8 0.6 add_convert_fusion
  105.4 0.7 copy.137
  (41 shorter events, 0.6 us)
Async XLA Ops:
  0.6 67.7 %copy-start = (bf16[2048,8]{0,1:T(8,128)(2,1)S(1)}, bf16[2048,8]{0,1:T(8,128)(2,1)}, u32[]{:S(2)}) copy-start(bf16[2048,8]{0,1:T(8,128)(2,1)} %param.37) | copy-start | bytes 98308
  0.6 40.1 %copy-start.11 = (f32[128,4,64]{0,2,1:T(8,128)S(1)}, f32[128,4,64]{0,2,1:T(8,128)}, u32[]{:S(2)}) copy-start(f32[128,4,64]{0,2,1:T(8,128)} %param.33) | copy-start | bytes 393220
  6.1 1.0 copy-start.5
  7.1 0.9 copy-start.6
  8.1 0.9 copy-start.7
  9.0 0.9 copy-start.8
  10.0 0.9 copy-start.9
  10.9 0.7 copy-start.10
  41.4 7.9 %copy-start.4 = (bf16[256,2048]{1,0:T(8,128)(2,1)S(1)}, bf16[256,2048]{1,0:T(8,128)(2,1)}, u32[]{:S(2)}) copy-start(bf16[256,2048]{1,0:T(8,128)(2,1)} %w.1) | copy-start | bytes 3145732
  41.4 25.8 %copy-start.13 = (f32[2048]{0:T(1024)S(1)}, f32[2048]{0:T(1024)}, u32[]{:S(2)}) copy-start(f32[2048]{0:T(1024)} %param.35) | copy-start | bytes 24580
  41.4 26.5 %copy-start.14 = (bf16[2048,4]{0,1:T(4,128)(2,1)S(1)}, bf16[2048,4]{0,1:T(4,128)(2,1)}, u32[]{:S(2)}) copy-start(bf16[2048,4]{0,1:T(4,128)(2,1)} %param.36) | copy-start | bytes 49156
  41.5 27.2 %copy-start.12 = (s32[128,2]{0,1:T(2,128)S(1)}, s32[128,2]{0,1:T(2,128)}, u32[]{:S(2)}) copy-start(s32[128,2]{0,1:T(2,128)} %param.38) | copy-start | bytes 3076
  41.5 27.7 %copy-start.1 = (bf16[2,2048,128]{2,1,0:T(8,128)(2,1)S(1)}, bf16[2,2048,128]{2,1,0:T(8,128)(2,1)}, u32[]{:S(2)}) copy-start(bf16[2,2048,128]{2,1,0:T(8,128)(2,1)} %wg.1) | copy-start | bytes 3145732
  69.1 1.2 %copy-start.2 = (bf16[2,2048,128]{2,1,0:T(8,128)(2,1)S(1)}, bf16[2,2048,128]{2,1,0:T(8,128)(2,1)}, u32[]{:S(2)}) copy-start(bf16[2,2048,128]{2,1,0:T(8,128)(2,1)} %wu.1) | copy-start | bytes 3145732
  70.4 1.2 %copy-start.3 = (bf16[2,128,2048]{2,1,0:T(8,128)(2,1)S(1)}, bf16[2,128,2048]{2,1,0:T(8,128)(2,1)}, u32[]{:S(2)}) copy-start(bf16[2,128,2048]{2,1,0:T(8,128)(2,1)} %wd.1) | copy-start | bytes 3145732
